TPU v7x, 32 devices: a whole 2x2x4 slice. The times are simulated.
32 devices in a mesh: tp: 8 (over z, x), dp: 4 (over y, core).
Axes of the slice: x: 2, y: 2, z: 4, core: 2. Of those that a mesh axis runs over, the one named last changes fastest.
Arguments:
- tokens: bfloat16 [112, 4096], P('tp', 'dp'), may hold values from -6 to 6
- w_query: bfloat16 [2, 4096, 4096], P(None, 'dp', 'tp'), may hold values from -0.09375 to 0.09375
- w_key: bfloat16 [2, 4096, 4096], P(None, 'dp', 'tp'), may hold values from -0.09375 to 0.09375
- w_value: bfloat16 [2, 4096, 4096], P(None, 'dp', 'tp'), may hold values from -0.09375 to 0.09375
- w_outgate: bfloat16 [2, 4096, 4096], P(None, 'dp', 'tp'), may hold values from -0.09375 to 0.09375
- w_ingate: bfloat16 [2, 4096, 32], P(None, 'dp'), may hold values from -0.09375 to 0.09375
- w_forget: bfloat16 [2, 4096, 32], P(None, 'dp'), may hold values from -0.09375 to 0.09375
- forget_bias: float32 [2, 32], P(None, 'tp'), may hold values from -2 to 3
- head_gain: float32 [2, 32, 128], P(None, 'tp'), may hold values from 0.1 to 1.9
- w_proj: bfloat16 [2, 4096, 4096], P(None, 'tp', 'dp'), may hold values from -0.09375 to 0.09375
- mem_matrix: float32 [2, 112, 32, 128, 128], P(None, 'dp', 'tp'), may hold values from -0.8 to 0.8
- mem_norm: float32 [2, 112, 32, 128], P(None, 'dp', 'tp'), may hold values from -1.2 to 1.2
- mem_max: float32 [2, 112, 32], P(None, 'dp', 'tp'), may hold values from -4 to 4
Outputs:
- result: bfloat16 [112, 4096], P('tp', 'dp')
- new_matrix: float32 [2, 112, 32, 128, 128], P(None, 'dp', 'tp')
- new_norm: float32 [2, 112, 32, 128], P(None, 'dp', 'tp')
- new_max: float32 [2, 112, 32], P(None, 'dp', 'tp')
All inputs are finite; a program needn't handle non-finite values.
Results may differ from a plain program's by a relative error of at most 0.017.
Values may be sent and summed in bfloat16 or wider, within the bound.
A program may use at most 128 MiB of HBM per device.

v0:
```python
import jax
import jax.numpy as jnp
from jax import lax
from jax.sharding import PartitionSpec as P

HEAD = 128
norm_eps = 1e-06
head_eps = 1e-05


def cell_update(queries, key_vecs, values, log_in, log_forget, matrix, normvec, maxval):
    max_next = jnp.maximum(log_forget + maxval, log_in)
    decays = jnp.exp(log_forget + maxval - max_next)
    weight_in = jnp.exp(log_in - max_next)
    matrix_new = (
        decays[..., None, None] * matrix
        + weight_in[..., None, None] * key_vecs[..., :, None] * values[..., None, :]
    )
    norm_new = decays[..., None] * normvec + weight_in[..., None] * key_vecs
    numerator = jnp.einsum("bhd,bhde->bhe", queries, matrix_new, precision=lax.Precision.HIGHEST)
    denominator = jnp.maximum(jnp.abs(jnp.sum(queries * norm_new, axis=-1)), 1.0)
    return (numerator / denominator[..., None], matrix_new, norm_new, max_next)


def head_norm(readout, gain, outgate):
    average = jnp.mean(readout, axis=-1, keepdims=True)
    variance = jnp.mean(jnp.square(readout - average), axis=-1, keepdims=True)
    normed = (readout - average) * lax.rsqrt(variance + head_eps) * gain
    return normed * jax.nn.sigmoid(outgate)


def mix_block(gathered, weights, states):
    w_query, w_key, w_value, w_outgate, w_ingate, w_forget, bias, gain, w_proj = weights
    matrix, normvec, maxval = states
    features = gathered.shape[1] * lax.axis_size("dp")
    squares = jnp.sum(jnp.square(gathered.astype(jnp.float32)), axis=1)
    heads_dev = bias.shape[0]
    head_start = lax.axis_index("tp") * heads_dev
    gate_in = lax.dynamic_slice_in_dim(w_ingate, head_start, heads_dev, 1)
    gate_forget = lax.dynamic_slice_in_dim(w_forget, head_start, heads_dev, 1)
    part_query = jnp.dot(gathered, w_query, preferred_element_type=jnp.float32)
    part_key = jnp.dot(gathered, w_key, preferred_element_type=jnp.float32)
    part_value = jnp.dot(gathered, w_value, preferred_element_type=jnp.float32)
    part_outgate = jnp.dot(gathered, w_outgate, preferred_element_type=jnp.float32)
    part_ingate = jnp.dot(gathered, gate_in, preferred_element_type=jnp.float32)
    part_forget = jnp.dot(gathered, gate_forget, preferred_element_type=jnp.float32)
    rows_dev = gathered.shape[0] // lax.axis_size("dp")
    totals = lax.psum(squares, "dp")
    own_sum = lax.dynamic_slice_in_dim(totals, lax.axis_index("dp") * rows_dev, rows_dev, 0)
    sum_query, sum_key, sum_value, sum_outgate, sum_ingate, sum_forget = (
        lax.psum_scatter(part_query, "dp", scatter_dimension=0, tiled=True),
        lax.psum_scatter(part_key, "dp", scatter_dimension=0, tiled=True),
        lax.psum_scatter(part_value, "dp", scatter_dimension=0, tiled=True),
        lax.psum_scatter(part_outgate, "dp", scatter_dimension=0, tiled=True),
        lax.psum_scatter(part_ingate, "dp", scatter_dimension=0, tiled=True),
        lax.psum_scatter(part_forget, "dp", scatter_dimension=0, tiled=True),
    )
    inv_scale = lax.rsqrt(own_sum / features + norm_eps)[:, None]
    head_shape = (rows_dev, heads_dev, HEAD)
    queries = (sum_query * inv_scale).reshape(head_shape)
    key_vecs = (sum_key * inv_scale * HEAD ** (-0.5)).reshape(head_shape)
    values = (sum_value * inv_scale).reshape(head_shape)
    outgate = (sum_outgate * inv_scale).reshape(head_shape)
    log_in = sum_ingate * inv_scale
    log_forget = jax.nn.log_sigmoid(sum_forget * inv_scale + bias[None, :])
    readout, matrix_new, norm_new, max_next = cell_update(
        queries, key_vecs, values, log_in, log_forget, matrix, normvec, maxval
    )
    hidden = head_norm(readout, gain[None], outgate).reshape(rows_dev, -1).astype(jnp.bfloat16)
    out_partial = jnp.dot(
        lax.all_gather(hidden, "dp", axis=0, tiled=True), w_proj, preferred_element_type=jnp.float32
    )
    return (out_partial, matrix_new, norm_new, max_next)


def on_device(
    tokens,
    w_query,
    w_key,
    w_value,
    w_outgate,
    w_ingate,
    w_forget,
    forget_bias,
    head_gain,
    w_proj,
    mem_matrix,
    mem_norm,
    mem_max,
):
    current = lax.all_gather(tokens, "tp", axis=0, tiled=True)
    matrix_list, norm_list, max_list = ([], [], [])
    block_total = w_query.shape[0]
    result = current
    for block_id in range(block_total):
        weights = (
            w_query[block_id],
            w_key[block_id],
            w_value[block_id],
            w_outgate[block_id],
            w_ingate[block_id],
            w_forget[block_id],
            forget_bias[block_id],
            head_gain[block_id],
            w_proj[block_id],
        )
        out_partial, matrix_out, norm_out, max_out = mix_block(
            current, weights, (mem_matrix[block_id], mem_norm[block_id], mem_max[block_id])
        )
        matrix_list.append(matrix_out)
        norm_list.append(norm_out)
        max_list.append(max_out)
        if block_id + 1 < block_total:
            current = lax.psum(out_partial, "tp").astype(jnp.bfloat16)
        else:
            result = lax.psum_scatter(
                out_partial.astype(jnp.bfloat16), "tp", scatter_dimension=0, tiled=True
            )
    return (result, jnp.stack(matrix_list), jnp.stack(norm_list), jnp.stack(max_list))


def solution(mesh):
    in_specs = (
        P("tp", "dp"),
        P(None, "dp", "tp"),
        P(None, "dp", "tp"),
        P(None, "dp", "tp"),
        P(None, "dp", "tp"),
        P(None, "dp", None),
        P(None, "dp", None),
        P(None, "tp"),
        P(None, "tp", None),
        P(None, "tp", "dp"),
        P(None, "dp", "tp", None, None),
        P(None, "dp", "tp", None),
        P(None, "dp", "tp"),
    )
    out_specs = (
        P("tp", "dp"),
        P(None, "dp", "tp", None, None),
        P(None, "dp", "tp", None),
        P(None, "dp", "tp"),
    )
    return jax.shard_map(
        on_device, mesh=mesh, in_specs=in_specs, out_specs=out_specs, check_vma=False
    )
```

profile of v0, /device:TPU:0, one launch (start us, length us, event | category | flops | bytes accessed | tf_op | source)
XLA Modules:
  0.0 243.8 jit_solution(15858441146114237513)
XLA Ops:
  0.7 32.9 %all-gather = bf16[8,14,1024]{2,1,0:T(8,128)(2,1)S(1)} all-gather(bf16[1,14,1024]{2,1,0:T(8,128)(2,1)} %bitcast.149), channel_id=1, replica_groups=mesh['tp'=8,'dp'=4] {'tp'}, dimensions={0}, use_global_device_ids=true | all-gather | bytes 258048 | tf_op jit(solution)/shard_map/all_gather | solution.py:91
  33.6 1.5 fusion.36
  35.2 1.5 fusion.38
  36.7 1.5 fusion.40
  38.2 2.4 fusion.42
  40.6 14.0 %fusion.93 = (f32[32,512]{1,0:T(8,128)S(1)}, f32[32,512]{1,0:T(8,128)S(1)}, f32[32,512]{1,0:T(8,128)S(1)}, f32[32,512]{1,0:T(8,128)S(1)}) fusion(f32[112,512]{1,0:T(8,128)S(1)} %fusion.36, f32[112,512]{1,0:T(8,128)} %fusion.42, f32[112,512]{1,0:T(8,128)S(1)} %fusion.38, f32[112,512]{1,0:T(8,128)S(1)} %fusion.40), kind=kCustom, calls=%all-reduce-scatter.10 | all-reduce-scatter fusion | flops 262145 | bytes 1180160
  54.6 1.3 collective-permute-start.1
  55.9 3.7 %collective-permute-start.2 = (f32[12,512]{1,0:T(8,128)S(1)}, f32[12,512]{1,0:T(8,128)S(1)}, u32[]{:S(2)}, u32[]{:S(2)}) collective-permute-start(f32[12,512]{1,0:T(8,128)S(1)} %slice.98), channel_id=1, source_target_pairs={{0,1},{1,2},{2,3},{4,5},{5,6},{6,7},{8,9},{9,10},{10,11},{12,13},{... | collective-permute-start | bytes 73736
  59.6 1.9 collective-permute-start
  61.6 1.9 collective-permute-start.3
  66.1 1.3 fusion.100
  68.1 5.8 %all-reduce.23 = (f32[112]{0:T(128)S(1)}, f32[112,4]{0,1:T(4,128)S(1)}, f32[112,4]{0,1:T(4,128)S(1)}) all-reduce(f32[112]{0:T(128)S(1)} %multiply_reduce_fusion.1, f32[112,4]{0,1:T(4,128)S(1)} %convolution_bitcast_fusion.1, f32[112,4]{0,1:T(4,128)S(1)} %convolution_bitcast_fusion), channel_id=1, replica_groups=mesh['tp'=8,'dp'=4] {'dp'}, use_global_device_ids=true, to_apply=%region_2.0 | all-reduce | flops 1008 | bytes 8064 | tf_op jit(solution)/shard_map/psum | solution.py:48
  79.7 9.2 %fusion.13 = f32[28,4,1,128]{3,2,1,0:T(1,128)S(1)} fusion(f32[28,4,128,1]{2,3,1,0:T(1,128)S(1)} %bitcast.148, f32[2,28,4,128,128]{4,3,2,1,0:T(8,128)} %param.23, f32[28,4,128]{2,1,0:T(4,128)S(1)} %mul.321, f32[28,4,128]{2,1,0:T(4,128)S(1)} %get-tuple-element.37, f32[28,4]{1,0:T(8,128)S(1)} %copy.41), kind=kOutput, calls=%fused_computation.6 | convolution fusion | flops 27525120 | bytes 7569856 | tf_op jit(solution)/shard_map/bhd,bhde->bhe/dot_general | solution.py:20
  89.4 5.4 %all-gather.1 = bf16[4,28,512]{2,1,0:T(8,128)(2,1)S(1)} all-gather(bf16[1,28,512]{2,1,0:T(8,128)(2,1)S(1)} %reshape.136), channel_id=1, replica_groups=mesh['tp'=8,'dp'=4] {'dp'}, dimensions={0}, use_global_device_ids=true | all-gather | bytes 143360 | tf_op jit(solution)/shard_map/all_gather | solution.py:71
  95.2 43.0 %all-reduce.27 = bf16[112,1024]{1,0:T(8,128)(2,1)S(1)} all-reduce(f32[112,1024]{1,0:T(8,128)S(1)} %fusion.34), channel_id=1, replica_groups=mesh['tp'=8,'dp'=4] {'tp'}, use_global_device_ids=true, to_apply=%region_11.12 | all-reduce | flops 114688 | bytes 688128 | tf_op jit(solution)/shard_map/psum | solution.py:114
  138.4 1.5 fusion.28
  139.9 1.5 fusion.30
  141.4 1.5 fusion.32
  143.0 1.5 fusion.26
  144.8 5.7 %all-reduce.22 = (f32[112]{0:T(128)S(1)}, f32[112,4]{0,1:T(4,128)S(1)}, f32[112,4]{0,1:T(4,128)S(1)}) all-reduce(f32[112]{0:T(128)S(1)} %multiply_reduce_fusion, f32[112,4]{0,1:T(4,128)S(1)} %fusion.72, f32[112,4]{0,1:T(4,128)S(1)} %fusion.70), channel_id=1, replica_groups=mesh['tp'=8,'dp'=4] {'dp'}, use_global_device_ids=true, to_apply=%region_14.15 | all-reduce | flops 1008 | bytes 8064 | tf_op jit(solution)/shard_map/psum | solution.py:48
  150.9 14.6 %fusion.92 = (f32[32,512]{1,0:T(8,128)S(1)}, f32[32,512]{1,0:T(8,128)S(1)}, f32[32,512]{1,0:T(8,128)S(1)}, f32[32,512]{1,0:T(8,128)S(1)}) fusion(f32[112,512]{1,0:T(8,128)S(1)} %fusion.26, f32[112,512]{1,0:T(8,128)S(1)} %fusion.32, f32[112,512]{1,0:T(8,128)S(1)} %fusion.28, f32[112,512]{1,0:T(8,128)S(1)} %fusion.30), kind=kCustom, calls=%all-reduce-scatter.9 | all-reduce-scatter fusion | flops 262145 | bytes 1180160
  165.5 1.3 collective-permute-start.5
  166.8 3.8 %collective-permute-start.6 = (f32[12,512]{1,0:T(8,128)S(1)}, f32[12,512]{1,0:T(8,128)S(1)}, u32[]{:S(2)}, u32[]{:S(2)}) collective-permute-start(f32[12,512]{1,0:T(8,128)S(1)} %slice.102), channel_id=1, source_target_pairs={{0,1},{1,2},{2,3},{4,5},{5,6},{6,7},{8,9},{9,10},{10,11},{12,13},{... | collective-permute-start | bytes 73736
  170.6 1.9 collective-permute-start.4
  172.6 2.1 collective-permute-start.7
  176.8 14.1 %multiply_add_fusion.1 = (f32[1,28,4,128,128]{4,3,2,1,0:T(8,128)}, f32[1,28,4,128,128]{4,3,2,1,0:T(8,128)}) fusion(f32[2,28,4,128,128]{4,3,2,1,0:T(8,128)} %param.23, f32[28,4,128]{2,1,0:T(4,128)S(1)} %mul.321, f32[28,4,128]{2,1,0:T(4,128)S(1)} %get-tuple-element.37, f32[28,4]{1,0:T(8,128)S(1)} %copy.41, f32[28,4,128]{2,1,0:T(4,128)S(1)} %mul.347, ...), kind=kLoop, calls=%fused_computation.8 | loop fusion | flops 11010048 | bytes 29590400 | tf_op jit(solution)/shard_map/add | solution.py:16
  190.9 6.9 %fusion.10 = f32[28,4,1,128]{3,2,1,0:T(1,128)S(1)} fusion(f32[28,4,128,1]{2,3,1,0:T(1,128)S(1)} %bitcast.147, f32[2,28,4,128,128]{4,3,2,1,0:T(8,128)S(1)} %bitcast.144, f32[28,4,128]{2,1,0:T(4,128)S(1)} %mul.347, f32[28,4,128]{2,1,0:T(4,128)S(1)} %get-tuple-element.33, f32[28,4]{1,0:T(8,128)S(1)} %copy.44), kind=kOutput, calls=%fused_computation.3 | convolution fusion | flops 27525120 | bytes 7585792 | tf_op jit(solution)/shard_map/bhd,bhde->bhe/dot_general | solution.py:20
  198.4 5.4 %all-gather.2 = bf16[4,28,512]{2,1,0:T(8,128)(2,1)S(1)} all-gather(bf16[1,28,512]{2,1,0:T(8,128)(2,1)S(1)} %reshape.138), channel_id=1, replica_groups=mesh['tp'=8,'dp'=4] {'dp'}, dimensions={0}, use_global_device_ids=true | all-gather | bytes 143360 | tf_op jit(solution)/shard_map/all_gather | solution.py:71
  203.9 1.5 convolution_convert_fusion
  205.4 21.2 %fusion.8 = bf16[16,1024]{1,0:T(8,128)(2,1)S(1)} fusion(bf16[112,1024]{1,0:T(8,128)(2,1)S(1)} %convolution_convert_fusion), kind=kCustom, calls=%all-reduce-scatter.8 | all-reduce-scatter fusion | flops 131073 | bytes 262656
  226.6 2.1 collective-permute-start.8
  228.9 13.4 %pad_maximum_fusion = f32[2,28,4,128,128]{4,3,2,1,0:T(8,128)} fusion(f32[1,28,4,128,128]{4,3,2,1,0:T(8,128)} %get-tuple-element.39, f32[1,28,4,128,128]{4,3,2,1,0:T(8,128)} %get-tuple-element.38), kind=kLoop, calls=%fused_computation | loop fusion | flops 3670016 | bytes 29360128 | tf_op jit(solution)/shard_map/stack | solution.py:119
  (105 shorter events, 12.8 us)
Async XLA Ops:
  0.6 64.3 %copy-start.2 = (bf16[2,1024,32]{1,2,0:T(8,128)(2,1)S(1)}, bf16[2,1024,32]{1,2,0:T(8,128)(2,1)}, u32[]{:S(2)}) copy-start(bf16[2,1024,32]{1,2,0:T(8,128)(2,1)} %param.18) | copy-start | bytes 393220
  0.6 78.8 %copy-start.1 = (f32[2,28,4,128]{3,2,1,0:T(4,128)S(1)}, f32[2,28,4,128]{3,2,1,0:T(4,128)}, u32[]{:S(2)}) copy-start(f32[2,28,4,128]{3,2,1,0:T(4,128)} %param.24) | copy-start | bytes 344068
  38.2 56.7 %copy-start = (bf16[2,512,1024]{2,1,0:T(8,128)(2,1)S(1)}, bf16[2,512,1024]{2,1,0:T(8,128)(2,1)}, u32[]{:S(2)}) copy-start(bf16[2,512,1024]{2,1,0:T(8,128)(2,1)} %param.22) | copy-start | bytes 6291460
  54.6 23.8 %collective-permute-start.1 = (f32[12,512]{1,0:T(8,128)S(1)}, f32[12,512]{1,0:T(8,128)S(1)}, u32[]{:S(2)}, u32[]{:S(2)}) collective-permute-start(f32[12,512]{1,0:T(8,128)S(1)} %slice.97), channel_id=1, source_target_pairs={{0,1},{1,2},{2,3},{4,5},{5,6},{6,7},{8,9},{9,10},{10,11},{12,13},{... | collective-permute-start | bytes 73736
  55.9 22.6 %collective-permute-start.2 = (f32[12,512]{1,0:T(8,128)S(1)}, f32[12,512]{1,0:T(8,128)S(1)}, u32[]{:S(2)}, u32[]{:S(2)}) collective-permute-start(f32[12,512]{1,0:T(8,128)S(1)} %slice.98), channel_id=1, source_target_pairs={{0,1},{1,2},{2,3},{4,5},{5,6},{6,7},{8,9},{9,10},{10,11},{12,13},{... | collective-permute-start | bytes 73736
  59.6 19.2 %collective-permute-start = (f32[12,512]{1,0:T(8,128)S(1)}, f32[12,512]{1,0:T(8,128)S(1)}, u32[]{:S(2)}, u32[]{:S(2)}) collective-permute-start(f32[12,512]{1,0:T(8,128)S(1)} %slice.96), channel_id=1, source_target_pairs={{0,1},{1,2},{2,3},{4,5},{5,6},{6,7},{8,9},{9,10},{10,11},{12,13},{... | collective-permute-start | bytes 73736
  61.6 17.4 %collective-permute-start.3 = (f32[12,512]{1,0:T(8,128)S(1)}, f32[12,512]{1,0:T(8,128)S(1)}, u32[]{:S(2)}, u32[]{:S(2)}) collective-permute-start(f32[12,512]{1,0:T(8,128)S(1)} %slice.99), channel_id=1, source_target_pairs={{0,1},{1,2},{2,3},{4,5},{5,6},{6,7},{8,9},{9,10},{10,11},{12,13},{... | collective-permute-start | bytes 73736
  79.7 71.0 %copy-start.3 = (f32[2,28,4]{1,2,0:T(4,128)S(1)}, f32[2,28,4]{1,2,0:T(4,128)}, u32[]{:S(2)}) copy-start(f32[2,28,4]{1,2,0:T(4,128)} %param.25) | copy-start | bytes 2692
  79.7 71.0 %copy-start.4 = (f32[4]{0:T(128)S(1)}, f32[4]{0:T(128)}, u32[]{:S(2)}) copy-start(f32[4]{0:T(128)} %get-tuple-element.52) | copy-start | bytes 52
  165.5 10.0 %collective-permute-start.5 = (f32[12,512]{1,0:T(8,128)S(1)}, f32[12,512]{1,0:T(8,128)S(1)}, u32[]{:S(2)}, u32[]{:S(2)}) collective-permute-start(f32[12,512]{1,0:T(8,128)S(1)} %slice.101), channel_id=1, source_target_pairs={{0,1},{1,2},{2,3},{4,5},{5,6},{6,7},{8,9},{9,10},{10,11},{12,13},{... | collective-permute-start | bytes 73736
  166.8 8.9 %collective-permute-start.6 = (f32[12,512]{1,0:T(8,128)S(1)}, f32[12,512]{1,0:T(8,128)S(1)}, u32[]{:S(2)}, u32[]{:S(2)}) collective-permute-start(f32[12,512]{1,0:T(8,128)S(1)} %slice.102), channel_id=1, source_target_pairs={{0,1},{1,2},{2,3},{4,5},{5,6},{6,7},{8,9},{9,10},{10,11},{12,13},{... | collective-permute-start | bytes 73736
  170.6 5.2 %collective-permute-start.4 = (f32[12,512]{1,0:T(8,128)S(1)}, f32[12,512]{1,0:T(8,128)S(1)}, u32[]{:S(2)}, u32[]{:S(2)}) collective-permute-start(f32[12,512]{1,0:T(8,128)S(1)} %slice.100), channel_id=1, source_target_pairs={{0,1},{1,2},{2,3},{4,5},{5,6},{6,7},{8,9},{9,10},{10,11},{12,13},{... | collective-permute-start | bytes 73736
  172.6 3.5 %collective-permute-start.7 = (f32[12,512]{1,0:T(8,128)S(1)}, f32[12,512]{1,0:T(8,128)S(1)}, u32[]{:S(2)}, u32[]{:S(2)}) collective-permute-start(f32[12,512]{1,0:T(8,128)S(1)} %slice.103), channel_id=1, source_target_pairs={{0,1},{1,2},{2,3},{4,5},{5,6},{6,7},{8,9},{9,10},{10,11},{12,13},{... | collective-permute-start | bytes 73736
  176.5 14.4 %slice-start = ((s8[14680064]{0:T(1024)(128)(4,1)}), s8[2097152]{0:T(1024)(128)(4,1)S(1)}, s32[]{:S(2)}) async-start(s8[14680064]{0:T(1024)(128)(4,1)} %bitcast.143), calls=%async_computation | async-start | bytes 4194304
  176.8 14.1 %slice-start.1 = ((s8[14680064]{0:T(1024)(128)(4,1)}), s8[4194304]{0:T(1024)(128)(4,1)S(1)}, s32[]{:S(2)}) async-start(s8[14680064]{0:T(1024)(128)(4,1)} %bitcast.143), calls=%async_computation.1 | async-start | bytes 8388608
  176.8 14.1 %slice-start.2 = ((s8[14680064]{0:T(1024)(128)(4,1)}), s8[4194304]{0:T(1024)(128)(4,1)S(1)}, s32[]{:S(2)}) async-start(s8[14680064]{0:T(1024)(128)(4,1)} %bitcast.143), calls=%async_computation.2 | async-start | bytes 8388608
  176.8 14.1 %slice-start.3 = ((s8[14680064]{0:T(1024)(128)(4,1)}), s8[4194304]{0:T(1024)(128)(4,1)S(1)}, s32[]{:S(2)}) async-start(s8[14680064]{0:T(1024)(128)(4,1)} %bitcast.143), calls=%async_computation.3 | async-start | bytes 8388608
  226.6 16.3 %collective-permute-start.8 = (bf16[14,1024]{1,0:T(8,128)(2,1)S(1)}, bf16[14,1024]{1,0:T(8,128)(2,1)S(1)}, u32[]{:S(2)}, u32[]{:S(2)}) collective-permute-start(bf16[14,1024]{1,0:T(8,128)(2,1)S(1)} %slice.104), channel_id=1, source_target_pairs={{0,4},{4,8},{8,12},{12,16},{16,20},{20,24},{24,28},{1,5},{5,9},{9,... | collective-permute-start | bytes 86024
where the time goes:
time: 245 us; the launch traced here: 244 us
  blocking collectives  148 us (60%)
  other arithmetic  31.9 us (13%)
  matrix products  31.7 us (13%)
  starting transfers between devices  20 us (8%)
  local copies, waits for them, and re-layouts  8.64 us (4%)
  between operations  3.34 us (1%)
    unnamed x3, blocking collectives  49.8 us
    psum x1, blocking collectives, on_device(): current = lax.psum(out_partial, 'tp').astype(jnp.bfloat16)  43 us
    all_gather x1, blocking collectives, on_device(): current = lax.all_gather(tokens, 'tp', axis=0, tiled=True)  32.9 us
    unnamed x9, starting transfers between devices  20 us
    dot_general x2, matrix products, cell_update(): jnp.einsum('bhd,bhde->bhe', queries, matrix_new, precision=lax.Precision....  16.1 us
    add x1, other arithmetic, cell_update(): decays[..., None, None] * matrix  14.1 us
    another operation x1, other arithmetic, on_device(): jnp.stack(matrix_list)  13.4 us
    psum x2, blocking collectives, mix_block(): totals = lax.psum(squares, 'dp')  11.6 us
  transfers between devices with their start and end apart: 9, of which 0 were waited for; matrix products, arithmetic and copies ran while one was open for 10% of the time, Pallas kernels for 0%

commit v1 on v0

--- a/solution.py
+++ b/solution.py
@@ -111,7 +111,7 @@
         norm_list.append(norm_out)
         max_list.append(max_out)
         if block_id + 1 < block_total:
-            current = lax.psum(out_partial, "tp").astype(jnp.bfloat16)
+            current = jnp.sum(lax.all_gather(out_partial, "tp"), axis=0).astype(jnp.bfloat16)
         else:
             result = lax.psum_scatter(
                 out_partial.astype(jnp.bfloat16), "tp", scatter_dimension=0, tiled=True

time: 245 us -> 283 us (1.16)
  waiting for transfers between devices: 0.02 us -> 66.2 us
  blocking collectives: 148 us -> 107 us
  between operations: 3.34 us -> 16.8 us
    all_gather x0 -> x1, waiting for transfers between devices: none -> 66.2 us  [on_device(): lax.all_gather(out_partial, 'tp')]
    psum x1 -> x0, blocking collectives: 43 us -> none  [on_device(): current = lax.psum(out_partial, 'tp').astype(jnp.bfloat16)]
  transfers between devices with their start and end apart: 9 -> 10, of which waited for: 0 -> 1; matrix products, arithmetic and copies ran while one was open for 10% -> 7% of each run, Pallas kernels for 0% -> 0%
where the time goes in v1:
time: 283 us; the launch traced here: 282 us
  blocking collectives  107 us (38%)
  waiting for transfers between devices  66.2 us (23%)
  other arithmetic  33.7 us (12%)
  matrix products  32.4 us (11%)
  starting transfers between devices  19.5 us (7%)
  between operations  16.8 us (6%)
  local copies, waits for them, and re-layouts  6.18 us (2%)
    all_gather x1, waiting for transfers between devices, on_device(): lax.all_gather(out_partial, 'tp')  66.2 us
    unnamed x3, blocking collectives  51.8 us
    all_gather x1, blocking collectives, on_device(): current = lax.all_gather(tokens, 'tp', axis=0, tiled=True)  32.9 us
    unnamed x9, starting transfers between devices  19.4 us
    dot_general x2, matrix products, cell_update(): jnp.einsum('bhd,bhde->bhe', queries, matrix_new, precision=lax.Precision....  16.1 us
    add x1, other arithmetic, cell_update(): decays[..., None, None] * matrix  14.1 us
    another operation x1, other arithmetic, on_device(): jnp.stack(matrix_list)  13.4 us
    psum x2, blocking collectives, mix_block(): totals = lax.psum(squares, 'dp')  11.6 us
  transfers between devices with their start and end apart: 10, of which 1 were waited for; matrix products, arithmetic and copies ran while one was open for 7% of the time, Pallas kernels for 0%

profile of v1, /device:TPU:0, one launch (start us, length us, event | category | flops | bytes accessed | tf_op | source)
XLA Modules:
  0.0 281.9 jit_solution(1711170090528397764)
XLA Ops:
  7.3 32.9 %all-gather.1 = bf16[8,14,1024]{2,1,0:T(8,128)(2,1)S(1)} all-gather(bf16[1,14,1024]{2,1,0:T(8,128)(2,1)} %bitcast.151), channel_id=1, replica_groups=mesh['tp'=8,'dp'=4] {'tp'}, dimensions={0}, use_global_device_ids=true | all-gather | bytes 258048 | tf_op jit(solution)/shard_map/all_gather | solution.py:91
  40.2 1.5 fusion.36
  41.8 1.5 fusion.38
  43.3 1.5 fusion.40
  44.9 2.4 fusion.42
  47.2 14.0 %fusion.93 = (f32[32,512]{1,0:T(8,128)S(1)}, f32[32,512]{1,0:T(8,128)S(1)}, f32[32,512]{1,0:T(8,128)S(1)}, f32[32,512]{1,0:T(8,128)S(1)}) fusion(f32[112,512]{1,0:T(8,128)S(1)} %fusion.36, f32[112,512]{1,0:T(8,128)} %fusion.42, f32[112,512]{1,0:T(8,128)S(1)} %fusion.38, f32[112,512]{1,0:T(8,128)S(1)} %fusion.40), kind=kCustom, calls=%all-reduce-scatter.10 | all-reduce-scatter fusion | flops 262145 | bytes 1180160
  61.2 1.3 collective-permute-start.1
  62.6 3.7 %collective-permute-start.2 = (f32[12,512]{1,0:T(8,128)S(1)}, f32[12,512]{1,0:T(8,128)S(1)}, u32[]{:S(2)}, u32[]{:S(2)}) collective-permute-start(f32[12,512]{1,0:T(8,128)S(1)} %slice.98), channel_id=1, source_target_pairs={{0,1},{1,2},{2,3},{4,5},{5,6},{6,7},{8,9},{9,10},{10,11},{12,13},{... | collective-permute-start | bytes 73736
  66.3 1.9 collective-permute-start
  68.2 1.9 collective-permute-start.3
  73.7 5.8 %all-reduce.23 = (f32[112]{0:T(128)S(1)}, f32[112,4]{0,1:T(4,128)S(1)}, f32[112,4]{0,1:T(4,128)S(1)}) all-reduce(f32[112]{0:T(128)S(1)} %multiply_reduce_fusion.1, f32[112,4]{0,1:T(4,128)S(1)} %convolution_bitcast_fusion.1, f32[112,4]{0,1:T(4,128)S(1)} %convolution_bitcast_fusion), channel_id=1, replica_groups=mesh['tp'=8,'dp'=4] {'dp'}, use_global_device_ids=true, to_apply=%region_2.0 | all-reduce | flops 1008 | bytes 8064 | tf_op jit(solution)/shard_map/psum | solution.py:48
  81.9 9.2 %fusion.13 = f32[28,4,1,128]{3,2,1,0:T(1,128)S(1)} fusion(f32[28,4,128,1]{2,3,1,0:T(1,128)S(1)} %bitcast.150, f32[2,28,4,128,128]{4,3,2,1,0:T(8,128)} %param.23, f32[28,4,128]{2,1,0:T(4,128)S(1)} %mul.321, f32[28,4,128]{2,1,0:T(4,128)S(1)} %get-tuple-element.37, f32[28,4]{1,0:T(8,128)S(1)} %copy.53), kind=kOutput, calls=%fused_computation.6 | convolution fusion | flops 27525120 | bytes 7569856 | tf_op jit(solution)/shard_map/bhd,bhde->bhe/dot_general | solution.py:20
  91.7 5.4 %all-gather.2 = bf16[4,28,512]{2,1,0:T(8,128)(2,1)S(1)} all-gather(bf16[1,28,512]{2,1,0:T(8,128)(2,1)S(1)} %reshape.137), channel_id=1, replica_groups=mesh['tp'=8,'dp'=4] {'dp'}, dimensions={0}, use_global_device_ids=true | all-gather | bytes 143360 | tf_op jit(solution)/shard_map/all_gather | solution.py:71
  99.5 66.2 %all-gather.6.cloned.1.call-done = f32[896,1024]{1,0:T(8,128)} async-done(((f32[112,1024]{1,0:T(8,128)}), f32[896,1024]{1,0:T(8,128)}) %all-gather.6.cloned.1.call-update) | async-done | bytes 3670032 | tf_op jit(solution)/shard_map/all_gather | solution.py:114
  165.7 2.4 reduce_sum.85
  168.2 1.5 fusion.28
  169.7 1.5 fusion.30
  171.3 1.5 fusion.32
  172.8 1.5 fusion.26
  174.7 5.7 %all-reduce.22 = (f32[112]{0:T(128)S(1)}, f32[112,4]{0,1:T(4,128)S(1)}, f32[112,4]{0,1:T(4,128)S(1)}) all-reduce(f32[112]{0:T(128)S(1)} %multiply_reduce_fusion, f32[112,4]{0,1:T(4,128)S(1)} %fusion.72, f32[112,4]{0,1:T(4,128)S(1)} %fusion.70), channel_id=1, replica_groups=mesh['tp'=8,'dp'=4] {'dp'}, use_global_device_ids=true, to_apply=%region_14.15 | all-reduce | flops 1008 | bytes 8064 | tf_op jit(solution)/shard_map/psum | solution.py:48
  180.7 14.2 %fusion.92 = (f32[32,512]{1,0:T(8,128)S(1)}, f32[32,512]{1,0:T(8,128)S(1)}, f32[32,512]{1,0:T(8,128)S(1)}, f32[32,512]{1,0:T(8,128)S(1)}) fusion(f32[112,512]{1,0:T(8,128)S(1)} %fusion.26, f32[112,512]{1,0:T(8,128)S(1)} %fusion.32, f32[112,512]{1,0:T(8,128)S(1)} %fusion.28, f32[112,512]{1,0:T(8,128)S(1)} %fusion.30), kind=kCustom, calls=%all-reduce-scatter.9 | all-reduce-scatter fusion | flops 262145 | bytes 1180160
  195.0 1.3 collective-permute-start.5
  196.3 4.0 %collective-permute-start.6 = (f32[12,512]{1,0:T(8,128)S(1)}, f32[12,512]{1,0:T(8,128)S(1)}, u32[]{:S(2)}, u32[]{:S(2)}) collective-permute-start(f32[12,512]{1,0:T(8,128)S(1)} %slice.102), channel_id=1, source_target_pairs={{0,1},{1,2},{2,3},{4,5},{5,6},{6,7},{8,9},{9,10},{10,11},{12,13},{... | collective-permute-start | bytes 73736
  200.3 1.9 collective-permute-start.4
  202.2 2.1 collective-permute-start.7
  206.5 14.1 %multiply_add_fusion.1 = (f32[1,28,4,128,128]{4,3,2,1,0:T(8,128)}, f32[1,28,4,128,128]{4,3,2,1,0:T(8,128)}) fusion(f32[2,28,4,128,128]{4,3,2,1,0:T(8,128)} %param.23, f32[28,4,128]{2,1,0:T(4,128)S(1)} %mul.321, f32[28,4,128]{2,1,0:T(4,128)S(1)} %get-tuple-element.37, f32[28,4]{1,0:T(8,128)S(1)} %copy.53, f32[28,4,128]{2,1,0:T(4,128)S(1)} %mul.347, ...), kind=kLoop, calls=%fused_computation.8 | loop fusion | flops 11010048 | bytes 29590400 | tf_op jit(solution)/shard_map/add | solution.py:16
  220.7 6.9 %fusion.10 = f32[28,4,1,128]{3,2,1,0:T(1,128)S(1)} fusion(f32[28,4,128,1]{2,3,1,0:T(1,128)S(1)} %bitcast.149, f32[2,28,4,128,128]{4,3,2,1,0:T(8,128)S(1)} %bitcast.145, f32[28,4,128]{2,1,0:T(4,128)S(1)} %mul.347, f32[28,4,128]{2,1,0:T(4,128)S(1)} %get-tuple-element.33, f32[28,4]{1,0:T(8,128)S(1)} %copy.56), kind=kOutput, calls=%fused_computation.3 | convolution fusion | flops 27525120 | bytes 7585792 | tf_op jit(solution)/shard_map/bhd,bhde->bhe/dot_general | solution.py:20
  228.1 5.4 %all-gather.3 = bf16[4,28,512]{2,1,0:T(8,128)(2,1)S(1)} all-gather(bf16[1,28,512]{2,1,0:T(8,128)(2,1)S(1)} %reshape.139), channel_id=1, replica_groups=mesh['tp'=8,'dp'=4] {'dp'}, dimensions={0}, use_global_device_ids=true | all-gather | bytes 143360 | tf_op jit(solution)/shard_map/all_gather | solution.py:71
  233.6 1.5 convolution_convert_fusion
  235.1 23.6 %fusion.8 = bf16[16,1024]{1,0:T(8,128)(2,1)S(1)} fusion(bf16[112,1024]{1,0:T(8,128)(2,1)S(1)} %convolution_convert_fusion), kind=kCustom, calls=%all-reduce-scatter.8 | all-reduce-scatter fusion | flops 131073 | bytes 262656
  258.7 1.3 collective-permute-start.8
  260.2 13.4 %pad_maximum_fusion = f32[2,28,4,128,128]{4,3,2,1,0:T(8,128)} fusion(f32[1,28,4,128,128]{4,3,2,1,0:T(8,128)} %get-tuple-element.39, f32[1,28,4,128,128]{4,3,2,1,0:T(8,128)} %get-tuple-element.38), kind=kLoop, calls=%fused_computation | loop fusion | flops 3670016 | bytes 29360128 | tf_op jit(solution)/shard_map/stack | solution.py:119
  (112 shorter events, 11.8 us)
Async XLA Ops:
  7.2 65.2 %copy-start.4 = (u32[32]{0:T(128)S(1)}, u32[32]{0:T(128)}, u32[]{:S(2)}) copy-start(u32[32]{0:T(128)} %constant.56) | copy-start | bytes 388
  7.2 63.1 %copy-start.5 = (f32[2,4]{1,0:T(2,128)S(1)}, f32[2,4]{1,0:T(2,128)}, u32[]{:S(2)}) copy-start(f32[2,4]{1,0:T(2,128)} %param.20) | copy-start | bytes 100
  7.2 72.4 %copy-start.3 = (f32[2,28,4]{1,2,0:T(4,128)S(1)}, f32[2,28,4]{1,2,0:T(4,128)}, u32[]{:S(2)}) copy-start(f32[2,28,4]{1,2,0:T(4,128)} %param.25) | copy-start | bytes 2692
  7.2 72.6 %copy-start.2 = (f32[2,4,128]{2,1,0:T(4,128)S(1)}, f32[2,4,128]{2,1,0:T(4,128)}, u32[]{:S(2)}) copy-start(f32[2,4,128]{2,1,0:T(4,128)} %param.21) | copy-start | bytes 12292
  7.2 74.5 %copy-start.1 = (f32[2,28,4,128]{3,2,1,0:T(4,128)S(1)}, f32[2,28,4,128]{3,2,1,0:T(4,128)}, u32[]{:S(2)}) copy-start(f32[2,28,4,128]{3,2,1,0:T(4,128)} %param.24) | copy-start | bytes 344068
  7.2 158.5 %all-gather.6.cloned.1.call-start = ((), (), s32[]{:S(2)}) async-start(), calls=%async_computation | async-start | bytes 4128768 | tf_op jit(solution)/shard_map/all_gather | solution.py:114
  44.8 52.3 %copy-start = (bf16[2,512,1024]{2,1,0:T(8,128)(2,1)S(1)}, bf16[2,512,1024]{2,1,0:T(8,128)(2,1)}, u32[]{:S(2)}) copy-start(bf16[2,512,1024]{2,1,0:T(8,128)(2,1)} %param.22) | copy-start | bytes 6291460
  61.2 37.0 %copy-start.6 = (u32[32]{0:T(128)S(1)}, u32[32]{0:T(128)}, u32[]{:S(2)}) copy-start(u32[32]{0:T(128)} %constant.104) | copy-start | bytes 388
  61.2 19.4 %collective-permute-start.1 = (f32[12,512]{1,0:T(8,128)S(1)}, f32[12,512]{1,0:T(8,128)S(1)}, u32[]{:S(2)}, u32[]{:S(2)}) collective-permute-start(f32[12,512]{1,0:T(8,128)S(1)} %slice.97), channel_id=1, source_target_pairs={{0,1},{1,2},{2,3},{4,5},{5,6},{6,7},{8,9},{9,10},{10,11},{12,13},{... | collective-permute-start | bytes 73736
  62.6 18.3 %collective-permute-start.2 = (f32[12,512]{1,0:T(8,128)S(1)}, f32[12,512]{1,0:T(8,128)S(1)}, u32[]{:S(2)}, u32[]{:S(2)}) collective-permute-start(f32[12,512]{1,0:T(8,128)S(1)} %slice.98), channel_id=1, source_target_pairs={{0,1},{1,2},{2,3},{4,5},{5,6},{6,7},{8,9},{9,10},{10,11},{12,13},{... | collective-permute-start | bytes 73736
  66.3 14.8 %collective-permute-start = (f32[12,512]{1,0:T(8,128)S(1)}, f32[12,512]{1,0:T(8,128)S(1)}, u32[]{:S(2)}, u32[]{:S(2)}) collective-permute-start(f32[12,512]{1,0:T(8,128)S(1)} %slice.96), channel_id=1, source_target_pairs={{0,1},{1,2},{2,3},{4,5},{5,6},{6,7},{8,9},{9,10},{10,11},{12,13},{... | collective-permute-start | bytes 73736
  68.2 13.1 %collective-permute-start.3 = (f32[12,512]{1,0:T(8,128)S(1)}, f32[12,512]{1,0:T(8,128)S(1)}, u32[]{:S(2)}, u32[]{:S(2)}) collective-permute-start(f32[12,512]{1,0:T(8,128)S(1)} %slice.99), channel_id=1, source_target_pairs={{0,1},{1,2},{2,3},{4,5},{5,6},{6,7},{8,9},{9,10},{10,11},{12,13},{... | collective-permute-start | bytes 73736
  195.0 10.2 %collective-permute-start.5 = (f32[12,512]{1,0:T(8,128)S(1)}, f32[12,512]{1,0:T(8,128)S(1)}, u32[]{:S(2)}, u32[]{:S(2)}) collective-permute-start(f32[12,512]{1,0:T(8,128)S(1)} %slice.101), channel_id=1, source_target_pairs={{0,1},{1,2},{2,3},{4,5},{5,6},{6,7},{8,9},{9,10},{10,11},{12,13},{... | collective-permute-start | bytes 73736
  196.3 9.0 %collective-permute-start.6 = (f32[12,512]{1,0:T(8,128)S(1)}, f32[12,512]{1,0:T(8,128)S(1)}, u32[]{:S(2)}, u32[]{:S(2)}) collective-permute-start(f32[12,512]{1,0:T(8,128)S(1)} %slice.102), channel_id=1, source_target_pairs={{0,1},{1,2},{2,3},{4,5},{5,6},{6,7},{8,9},{9,10},{10,11},{12,13},{... | collective-permute-start | bytes 73736
  200.3 5.2 %collective-permute-start.4 = (f32[12,512]{1,0:T(8,128)S(1)}, f32[12,512]{1,0:T(8,128)S(1)}, u32[]{:S(2)}, u32[]{:S(2)}) collective-permute-start(f32[12,512]{1,0:T(8,128)S(1)} %slice.100), channel_id=1, source_target_pairs={{0,1},{1,2},{2,3},{4,5},{5,6},{6,7},{8,9},{9,10},{10,11},{12,13},{... | collective-permute-start | bytes 73736
  202.2 3.5 %collective-permute-start.7 = (f32[12,512]{1,0:T(8,128)S(1)}, f32[12,512]{1,0:T(8,128)S(1)}, u32[]{:S(2)}, u32[]{:S(2)}) collective-permute-start(f32[12,512]{1,0:T(8,128)S(1)} %slice.103), channel_id=1, source_target_pairs={{0,1},{1,2},{2,3},{4,5},{5,6},{6,7},{8,9},{9,10},{10,11},{12,13},{... | collective-permute-start | bytes 73736
  206.1 14.5 %slice-start = ((s8[14680064]{0:T(1024)(128)(4,1)}), s8[2097152]{0:T(1024)(128)(4,1)S(1)}, s32[]{:S(2)}) async-start(s8[14680064]{0:T(1024)(128)(4,1)} %bitcast.144), calls=%async_computation.1 | async-start | bytes 4194304
  206.5 14.2 %slice-start.1 = ((s8[14680064]{0:T(1024)(128)(4,1)}), s8[4194304]{0:T(1024)(128)(4,1)S(1)}, s32[]{:S(2)}) async-start(s8[14680064]{0:T(1024)(128)(4,1)} %bitcast.144), calls=%async_computation.2 | async-start | bytes 8388608
  206.5 14.2 %slice-start.2 = ((s8[14680064]{0:T(1024)(128)(4,1)}), s8[4194304]{0:T(1024)(128)(4,1)S(1)}, s32[]{:S(2)}) async-start(s8[14680064]{0:T(1024)(128)(4,1)} %bitcast.144), calls=%async_computation.3 | async-start | bytes 8388608
  206.5 14.2 %slice-start.3 = ((s8[14680064]{0:T(1024)(128)(4,1)}), s8[4194304]{0:T(1024)(128)(4,1)S(1)}, s32[]{:S(2)}) async-start(s8[14680064]{0:T(1024)(128)(4,1)} %bitcast.144), calls=%async_computation.4 | async-start | bytes 8388608
  258.7 15.5 %collective-permute-start.8 = (bf16[14,1024]{1,0:T(8,128)(2,1)S(1)}, bf16[14,1024]{1,0:T(8,128)(2,1)S(1)}, u32[]{:S(2)}, u32[]{:S(2)}) collective-permute-start(bf16[14,1024]{1,0:T(8,128)(2,1)S(1)} %slice.104), channel_id=1, source_target_pairs={{0,4},{4,8},{8,12},{12,16},{16,20},{20,24},{24,28},{1,5},{5,9},{9,... | collective-permute-start | bytes 86024
Sparse Core Ops, SparseCore 0:
  98.4 67.2 all-gather.5
